TPU v7x, 32 devices: a whole 2x2x4 slice. The times are simulated.
32 devices in a mesh: ep: 8 (over z, y), tp: 4 (over x, core).
Axes of the slice: x: 2, y: 2, z: 4, core: 2. Of those that a mesh axis runs over, the one named last changes fastest.
Arguments:
- tokens: bfloat16 [1024, 2048], P('ep'), may hold values from -6 to 6
- cotangent: bfloat16 [1024, 2048], P('ep'), may hold values from -2 to 2
- route_weights: float32 [1024, 2], P('ep'), may hold values from 0.25 to 2.5
- routes: int32 [1024, 2], P('ep'), may hold values from 0 to 7, all different within a row; in each aligned block of 128 rows (0 to 127, 128 to 255, ...) at most 64 rows name the same one
- gate_proj: bfloat16 [8, 2048, 512], P('ep', None, 'tp'), may hold values from -0.125 to 0.125
- up_proj: bfloat16 [8, 2048, 512], P('ep', None, 'tp'), may hold values from -0.125 to 0.125
- down_proj: bfloat16 [8, 512, 2048], P('ep', 'tp'), may hold values from -0.25 to 0.25
- shared_down: bfloat16 [2048, 512], P(None, 'tp'), may hold values from -0.25 to 0.25
- shared_hidden: bfloat16 [1024, 512], P('ep', 'tp'), may hold values from -0.29882812 to 0.29882812
Outputs:
- tokens_grad: bfloat16 [1024, 2048], P('ep', 'tp')
- weights_grad: float32 [1024, 2], P('ep')
- gate_proj_grad: bfloat16 [8, 2048, 512], P('ep', None, 'tp')
- up_proj_grad: bfloat16 [8, 2048, 512], P('ep', None, 'tp')
- down_proj_grad: bfloat16 [8, 512, 2048], P('ep', 'tp')
- hidden_grad: bfloat16 [1024, 512], P('ep', 'tp')
- shared_grad: float32 [2048, 512], P('ep', 'tp')
Inputs may be any that keep to these rules, and one draw needn't show every extreme that they name: `routes`: in each aligned block of 128 rows no expert is named more than 64 times, a bound that some block reaches; the 2 experts of a row differ.
All inputs are finite; a program needn't handle non-finite values.
Results may differ from a plain program's by a relative error of at most 0.012.
Values may be sent and summed in bfloat16 or wider, within the bound.
A program may use at most 64 MiB of HBM per device.

v0:
```python
import jax
import jax.numpy as jnp
from jax import lax
from jax.sharding import PartitionSpec as P


def shards(
    tokens,
    cotangent,
    route_weights,
    routes,
    gate_proj,
    up_proj,
    down_proj,
    shared_down,
    shared_hidden,
):
    tok_rows, feat_width = tokens.shape
    top_count = routes.shape[1]
    exp_local = gate_proj.shape[0]
    ep_size = lax.axis_size("ep")
    tp_size = lax.axis_size("tp")
    exp_total = exp_local * ep_size
    capacity = 2 * tok_rows * top_count // exp_total
    quarter = feat_width // tp_size
    filled = exp_total * capacity
    flat_routes = routes.reshape(-1)
    one_hot = (flat_routes[:, None] == jnp.arange(exp_total, dtype=jnp.int32)[None, :]).astype(
        jnp.int32
    )
    rank_in = jnp.sum((jnp.cumsum(one_hot, axis=0) - one_hot) * one_hot, axis=1)
    slot_ids = flat_routes * capacity + rank_in
    route_owner = jnp.arange(flat_routes.shape[0], dtype=jnp.int32) // top_count
    owner_ids = jnp.full((filled,), tok_rows, jnp.int32).at[slot_ids].set(route_owner)
    sent_weights = (
        jnp.zeros((filled,), jnp.bfloat16)
        .at[slot_ids]
        .set(route_weights.reshape(-1).astype(jnp.bfloat16))
    )
    first_col = lax.axis_index("tp") * quarter
    own_rows = lax.dynamic_slice_in_dim(tokens, first_col, quarter, 1)
    own_grads = lax.dynamic_slice_in_dim(cotangent, first_col, quarter, 1)
    sent_rows = jnp.take(own_rows, owner_ids, axis=0, mode="fill", fill_value=0)
    sent_grads = jnp.take(own_grads, owner_ids, axis=0, mode="fill", fill_value=0)
    got_rows, got_grads, got_weights = (
        lax.all_to_all(sent_rows, "ep", split_axis=0, concat_axis=0, tiled=True),
        lax.all_to_all(sent_grads, "ep", split_axis=0, concat_axis=0, tiled=True),
        lax.all_to_all(sent_weights, "ep", split_axis=0, concat_axis=0, tiled=True),
    )
    got_rows, got_grads = (
        lax.all_gather(got_rows, "tp", axis=1, tiled=True),
        lax.all_gather(got_grads, "tp", axis=1, tiled=True),
    )
    slot_rows = got_rows.reshape(ep_size, exp_local, capacity, feat_width)
    slot_grads = got_grads.reshape(ep_size, exp_local, capacity, feat_width)
    weight_col = got_weights.reshape(ep_size, exp_local, capacity, 1).astype(jnp.float32)
    gate = jnp.einsum("secd,edf->secf", slot_rows, gate_proj, preferred_element_type=jnp.float32)
    upper = jnp.einsum("secd,edf->secf", slot_rows, up_proj, preferred_element_type=jnp.float32)
    active = jax.nn.silu(gate)
    hidden = (active * upper).astype(jnp.bfloat16)
    backed = jnp.einsum("secd,efd->secf", slot_grads, down_proj, preferred_element_type=jnp.float32)
    gate_share = jnp.sum(hidden.astype(jnp.float32) * backed, axis=3)
    d_hidden = weight_col * backed
    sigma = jax.nn.sigmoid(gate)
    d_gate = (d_hidden * upper * sigma * (1.0 + gate * (1.0 - sigma))).astype(jnp.bfloat16)
    d_up = (d_hidden * active).astype(jnp.bfloat16)
    scaled = (weight_col * slot_grads).astype(jnp.bfloat16)
    down_proj_grad = jnp.einsum(
        "secf,secd->efd", hidden, scaled, preferred_element_type=jnp.float32
    ).astype(jnp.bfloat16)
    gate_proj_grad = jnp.einsum(
        "secd,secf->edf", slot_rows, d_gate, preferred_element_type=jnp.float32
    ).astype(jnp.bfloat16)
    up_proj_grad = jnp.einsum(
        "secd,secf->edf", slot_rows, d_up, preferred_element_type=jnp.float32
    ).astype(jnp.bfloat16)
    partial_value = jnp.einsum(
        "secf,edf->secd", d_gate, gate_proj, preferred_element_type=jnp.float32
    )
    partial_value = partial_value + jnp.einsum(
        "secf,edf->secd", d_up, up_proj, preferred_element_type=jnp.float32
    )
    gate_whole = lax.psum(gate_share, "tp")
    input_cols = lax.psum_scatter(
        partial_value.astype(jnp.bfloat16), "tp", scatter_dimension=3, tiled=True
    )
    back_cols, back_gate = (
        lax.all_to_all(
            input_cols.reshape(filled, quarter), "ep", split_axis=0, concat_axis=0, tiled=True
        ),
        lax.all_to_all(
            gate_whole.astype(jnp.bfloat16).reshape(filled),
            "ep",
            split_axis=0,
            concat_axis=0,
            tiled=True,
        ),
    )
    picked = back_cols[slot_ids].reshape(tok_rows, top_count, quarter)
    tokens_grad = jnp.sum(picked.astype(jnp.float32), axis=1).astype(jnp.bfloat16)
    weights_grad = back_gate[slot_ids].astype(jnp.float32).reshape(tok_rows, top_count)
    hidden_grad = jnp.dot(cotangent, shared_down, preferred_element_type=jnp.float32).astype(
        jnp.bfloat16
    )
    shared_grad = lax.psum_scatter(
        jnp.einsum("td,th->dh", cotangent, shared_hidden, preferred_element_type=jnp.float32),
        "ep",
        scatter_dimension=0,
        tiled=True,
    )
    return (
        tokens_grad,
        weights_grad,
        gate_proj_grad,
        up_proj_grad,
        down_proj_grad,
        hidden_grad,
        shared_grad,
    )


def solution(mesh):
    in_specs = (
        P("ep", None),
        P("ep", None),
        P("ep", None),
        P("ep", None),
        P("ep", None, "tp"),
        P("ep", None, "tp"),
        P("ep", "tp", None),
        P(None, "tp"),
        P("ep", "tp"),
    )
    out_specs = (
        P("ep", "tp"),
        P("ep", None),
        P("ep", None, "tp"),
        P("ep", None, "tp"),
        P("ep", "tp", None),
        P("ep", "tp"),
        P("ep", "tp"),
    )
    return jax.shard_map(shards, mesh=mesh, in_specs=in_specs, out_specs=out_specs, check_vma=False)
```

profile of v0, /device:TPU:0, one launch (start us, length us, event | category | flops | bytes accessed | tf_op | source)
XLA Modules:
  0.0 198.5 jit_solution(4977490238628618403)
XLA Ops:
  7.2 0.7 broadcast_multiply_fusion
  8.0 0.8 copy.27
  10.3 1.4 scatter_custom_fusion.1
  11.7 0.9 constant_dynamic-slice_fusion
  12.6 0.9 constant_dynamic-slice_fusion.1
  13.6 2.0 gather_fusion.2
  15.5 2.0 gather_fusion.3
  17.7 21.7 %all_to_all.58 = bf16[8,64,512]{2,1,0:T(8,128)(2,1)} all-to-all(bf16[8,64,512]{2,1,0:T(8,128)(2,1)S(1)} %bitcast.120), channel_id=1, replica_groups=mesh['ep'=8,'tp'=4] {'ep'}, dimensions={0} | all-to-all | bytes 1048576 | tf_op jit(solution)/shard_map/all_to_all | solution.py:46
  39.5 17.8 %all_to_all.59 = bf16[8,64,512]{2,1,0:T(8,128)(2,1)} all-to-all(bf16[8,64,512]{2,1,0:T(8,128)(2,1)S(1)} %bitcast.119), channel_id=1, replica_groups=mesh['ep'=8,'tp'=4] {'ep'}, dimensions={0} | all-to-all | bytes 1048576 | tf_op jit(solution)/shard_map/all_to_all | solution.py:47
  57.6 2.2 %scatter_custom_fusion = bf16[512]{0:T(512)(128)(2,1)S(1)} fusion(s32[256]{0:T(256)S(1)} %bitcast.130, bf16[256]{0:T(256)(128)(2,1)S(1)} %reshape.210, bf16[]{:T(256)} %constant.23.clone.1), kind=kCustom, calls=%fused_computation.63 | custom fusion | bytes 1026 | tf_op jit(solution)/shard_map/scatter | solution.py:38
  59.9 9.9 %all_to_all.60 = bf16[8,64,1]{1,2,0:T(2,128)(2,1)S(1)} all-to-all(bf16[8,64,1]{1,2,0:T(2,128)(2,1)S(1)} %all_to_all.52), channel_id=1, replica_groups=mesh['ep'=8,'tp'=4] {'ep'}, dimensions={0} | all-to-all | bytes 2048 | tf_op jit(solution)/shard_map/all_to_all | solution.py:48
  69.8 2.8 %convolution_bitcast_fusion.3 = f32[8,1,64,128]{3,2,0,1:T(8,128)S(1)} fusion(bf16[8,64,2048]{2,1,0:T(8,128)(2,1)} %bitcast.115, bf16[1,2048,128]{2,1,0:T(8,128)(2,1)S(1)} %copy-done), kind=kOutput, calls=%fused_computation.19 | convolution fusion | flops 268435456 | bytes 2883584 | tf_op jit(solution)/shard_map/secd,edf->secf/dot_general | solution.py:57
  72.6 1.4 convolution_bitcast_fusion.4
  74.0 11.3 %all-gather.3.cloned.1.call-done = bf16[512,2048]{1,0:T(8,128)(2,1)} async-done(((bf16[512,512]{1,0:T(8,128)(2,1)}), bf16[512,2048]{1,0:T(8,128)(2,1)}) %all-gather.3.cloned.1.call-update) | async-done | bytes 2097168 | tf_op jit(solution)/shard_map/all_gather | solution.py:52
  85.3 3.1 %multiply_reduce_fusion = (f32[8,64]{1,0:T(8,128)S(1)}, bf16[8,1,64,128]{3,2,0,1:T(8,128)(2,1)}, bf16[8,1,64,128]{3,2,0,1:T(8,128)(2,1)S(1)}, bf16[8,64,128]{2,1,0:T(8,128)(2,1)S(1)}) fusion(f32[8,1,64,128]{3,2,0,1:T(8,128)} %convolution_bitcast_fusion.4, f32[8,1,64,128]{3,2,0,1:T(8,128)S(1)} %convolution_bitcast_fusion.3, f32[8,64]{1,0:T(8,128)S(1)} %bitcast.126, ...), kind=kOutput, calls=%fused_computation.31 | convolution fusion | flops 269680128 | bytes 3543040 | tf_op jit(solution)/shard_map/secd,efd->secf/dot_general | solution.py:61
  88.5 0.7 fusion.8
  89.2 2.0 %fusion = bf16[8,1,64,2048]{3,2,0,1:T(8,128)(2,1)} fusion(f32[8,64,2048]{2,1,0:T(8,128)S(1)} %fusion.8, bf16[8,64,128]{2,1,0:T(8,128)(2,1)S(1)} %get-tuple-element.32, bf16[1,2048,128]{2,1,0:T(8,128)(2,1)S(1)} %copy-done.3), kind=kOutput, calls=%fused_computation.8 | convolution fusion | flops 270532608 | bytes 6946816 | tf_op jit(solution)/shard_map/secf,edf->secd/dot_general | solution.py:80
  91.3 1.0 copy-done.2
  92.2 1.3 fusion.28
  93.6 5.9 %psum.7 = bf16[8,1,64]{2,0,1:T(8,128)(2,1)S(1)} all-reduce(f32[8,1,64]{2,0,1:T(8,128)S(1)} %bitcast.132), channel_id=1, replica_groups=mesh['ep'=8,'tp'=4] {'tp'}, use_global_device_ids=true, to_apply=%region_8.10 | all-reduce | flops 512 | bytes 3072 | tf_op jit(solution)/shard_map/psum | solution.py:83
  99.5 12.0 %all_to_all.61 = bf16[8,64,1]{1,2,0:T(2,128)(2,1)S(1)} all-to-all(bf16[8,64,1]{1,2,0:T(2,128)(2,1)S(1)} %copy.31), channel_id=1, replica_groups=mesh['ep'=8,'tp'=4] {'ep'}, dimensions={0} | all-to-all | bytes 2048 | tf_op jit(solution)/shard_map/all_to_all | solution.py:91
  111.4 11.1 %reduce-scatter.3.cloned.1.call-done = bf16[8,1,64,512]{3,2,0,1:T(8,128)(2,1)} async-done(((bf16[8,1,64,2048]{3,2,0,1:T(8,128)(2,1)}), bf16[8,1,64,512]{3,2,0,1:T(8,128)(2,1)}) %reduce-scatter.3.cloned.1.call-update) | async-done | bytes 524304 | tf_op jit(solution)/shard_map/reduce_scatter | solution.py:84
  122.6 5.5 %all-to-all-start.3 = ((bf16[8,64,512]{2,1,0:T(8,128)(2,1)}), bf16[8,64,512]{2,1,0:T(8,128)(2,1)S(1)}, u32[]{:S(2)}, u32[]{:S(2)}) async-start(bf16[8,64,512]{2,1,0:T(8,128)(2,1)} %bitcast.125), calls=%async_computation.4 | async-start | bytes 1048576 | tf_op jit(solution)/shard_map/all_to_all | solution.py:88
  128.1 2.1 %convolution_convert_fusion = bf16[128,128]{1,0:T(8,128)(2,1)} fusion(bf16[128,2048]{1,0:T(8,128)(2,1)} %param.12, bf16[2048,128]{1,0:T(8,128)(2,1)} %param.18), kind=kOutput, calls=%fused_computation.22 | convolution fusion | flops 67125248 | bytes 1081344 | tf_op jit(solution)/shard_map/dot_general | solution.py:102
  130.2 3.0 %fusion.4 = bf16[1,128,2048]{2,1,0:T(8,128)(2,1)} fusion(bf16[8,64,2048]{2,1,0:T(8,128)(2,1)} %bitcast.122, f32[8,64]{1,0:T(8,128)S(1)} %bitcast.127, bf16[8,1,64,128]{3,2,0,1:T(8,128)(2,1)S(1)} %copy-done.6), kind=kOutput, calls=%fused_computation.15 | convolution fusion | flops 271843328 | bytes 2754560 | tf_op jit(solution)/shard_map/secf,secd->efd/dot_general | solution.py:68
  133.2 1.6 fusion.6
  134.8 1.6 fusion.5
  136.5 1.9 gather_fusion.1
  139.2 7.2 %all-to-all-done.3 = bf16[8,64,512]{2,1,0:T(8,128)(2,1)S(1)} async-done(((bf16[8,64,512]{2,1,0:T(8,128)(2,1)}), bf16[8,64,512]{2,1,0:T(8,128)(2,1)S(1)}, u32[]{:S(2)}, u32[]{:S(2)}) %all-to-all-start.3) | async-done | bytes 524320 | tf_op jit(solution)/shard_map/all_to_all | solution.py:88
  146.4 1.2 gather_fusion
  147.6 1.3 reduce_sum.36
  148.9 43.0 %reduce-scatter.5.cloned.1.call-done = f32[256,128]{1,0:T(8,128)} async-done(((f32[2048,128]{1,0:T(8,128)}), f32[256,128]{1,0:T(8,128)}) %reduce-scatter.5.cloned.1.call-update) | async-done | bytes 131088 | tf_op jit(solution)/shard_map/reduce_scatter | solution.py:105
  (54 shorter events, 3.3 us)
Async XLA Ops:
  7.2 62.7 %copy-start = (bf16[1,2048,128]{2,1,0:T(8,128)(2,1)S(1)}, bf16[1,2048,128]{2,1,0:T(8,128)(2,1)}, u32[]{:S(2)}) copy-start(bf16[1,2048,128]{2,1,0:T(8,128)(2,1)} %param.15) | copy-start | bytes 1572868
  7.2 62.6 %all-gather.5.cloned.1.call-start = ((), (), s32[]{:S(2)}) async-start(), calls=%async_computation.8 | async-start | bytes 2621440 | tf_op jit(solution)/shard_map/all_gather | solution.py:51
  17.7 39.7 %copy-start.8 = (f32[128,2]{0,1:T(2,128)S(1)}, f32[128,2]{0,1:T(2,128)}, u32[]{:S(2)}) copy-start(f32[128,2]{0,1:T(2,128)} %param.13) | copy-start | bytes 3076
  39.4 45.9 %all-gather.3.cloned.1.call-start = ((), (), s32[]{:S(2)}) async-start(), calls=%async_computation.7 | async-start | bytes 2621440 | tf_op jit(solution)/shard_map/all_gather | solution.py:52
  39.5 33.1 %copy-start.3 = (bf16[1,2048,128]{2,1,0:T(8,128)(2,1)S(1)}, bf16[1,2048,128]{2,1,0:T(8,128)(2,1)}, u32[]{:S(2)}) copy-start(bf16[1,2048,128]{2,1,0:T(8,128)(2,1)} %param.16) | copy-start | bytes 1572868
  57.3 65.3 %reduce-scatter.3.cloned.1.call-start = ((), (), s32[]{:S(2)}) async-start(), calls=%async_computation.9 | async-start | bytes 2621440 | tf_op jit(solution)/shard_map/reduce_scatter | solution.py:84
  69.8 2.8 %copy-start.1 = (bf16[512,2048]{1,0:T(8,128)(2,1)S(1)}, bf16[512,2048]{1,0:T(8,128)(2,1)}, u32[]{:S(2)}) copy-start(bf16[512,2048]{1,0:T(8,128)(2,1)} %all-gather.5.cloned.1.call-done) | copy-start | bytes 6291460
  88.5 0.7 copy-start.4
  91.2 1.0 copy-start.2
  91.2 1.0 copy-start.7
  91.2 39.0 %copy-start.6 = (bf16[8,1,64,128]{3,2,0,1:T(8,128)(2,1)S(1)}, bf16[8,1,64,128]{3,2,0,1:T(8,128)(2,1)}, u32[]{:S(2)}) copy-start(bf16[8,1,64,128]{3,2,0,1:T(8,128)(2,1)} %get-tuple-element.30) | copy-start | bytes 393220
  91.2 100.7 %reduce-scatter.5.cloned.1.call-start = ((), (), s32[]{:S(2)}) async-start(), calls=%async_computation.10 | async-start | bytes 1179648 | tf_op jit(solution)/shard_map/reduce_scatter | solution.py:105
  122.6 23.8 %all-to-all-start.3 = ((bf16[8,64,512]{2,1,0:T(8,128)(2,1)}), bf16[8,64,512]{2,1,0:T(8,128)(2,1)S(1)}, u32[]{:S(2)}, u32[]{:S(2)}) async-start(bf16[8,64,512]{2,1,0:T(8,128)(2,1)} %bitcast.125), calls=%async_computation.4 | async-start | bytes 1048576 | tf_op jit(solution)/shard_map/all_to_all | solution.py:88
  128.1 5.2 %copy-start.5 = (bf16[8,1,64,128]{3,2,0,1:T(8,128)(2,1)S(1)}, bf16[8,1,64,128]{3,2,0,1:T(8,128)(2,1)}, u32[]{:S(2)}) copy-start(bf16[8,1,64,128]{3,2,0,1:T(8,128)(2,1)} %copy-done.4) | copy-start | bytes 393220
Sparse Core Ops, SparseCore 0:
  39.6 21.5 all-gather.4
  62.7 22.5 all-gather.2
  91.3 31.1 reduce-scatter.2
  126.4 65.4 reduce-scatter.4
where the time goes:
time: 199 us; the launch traced here: 198 us
  waiting for transfers between devices  72.6 us (36%)
  blocking collectives  67.3 us (34%)
  matrix products  19.6 us (10%)
  local copies, waits for them, and re-layouts  16.3 us (8%)
  between operations  14 us (7%)
  starting transfers between devices  5.68 us (3%)
  other arithmetic  2.98 us (1%)
    reduce_scatter x1, waiting for transfers between devices, shards(): lax.psum_scatter(jnp.einsum('td,th->dh', cotangent, shared_hidden, prefer...  43 us
    all_to_all x1, blocking collectives, shards(): lax.all_to_all(sent_rows, 'ep', split_axis=0, concat_axis=0, tiled=True)  21.7 us
    all_to_all x1, blocking collectives, shards(): lax.all_to_all(sent_grads, 'ep', split_axis=0, concat_axis=0, tiled=True)  17.8 us
    all_to_all x1, blocking collectives, shards(): lax.all_to_all(gate_whole.astype(jnp.bfloat16).reshape(filled), 'ep', spl...  12 us
    all_gather x1, waiting for transfers between devices, shards(): lax.all_gather(got_grads, 'tp', axis=1, tiled=True)  11.3 us
    reduce_scatter x1, waiting for transfers between devices, shards(): lax.psum_scatter(partial_value.astype(jnp.bfloat16), 'tp', scatter_dimens...  11.1 us
    all_to_all x1, blocking collectives, shards(): lax.all_to_all(sent_weights, 'ep', split_axis=0, concat_axis=0, tiled=True)  9.92 us
    all_to_all x1, waiting for transfers between devices, shards(): lax.all_to_all(input_cols.reshape(filled, quarter), 'ep', split_axis=0, c...  7.17 us
  transfers between devices with their start and end apart: 5, of which 4 were waited for; matrix products, arithmetic and copies ran while one was open for 11% of the time, Pallas kernels for 0%

commit v1 on v0

--- a/solution.py
+++ b/solution.py
@@ -1,10 +1,461 @@
+import functools
+
 import jax
 import jax.numpy as jnp
 from jax import lax
+from jax.experimental import pallas as pl
+from jax.experimental.pallas import tpu as pltpu
 from jax.sharding import PartitionSpec as P
 
-
-def shards(
+MESH = pl.DeviceIdType.MESH
+BF = jnp.bfloat16
+F32 = jnp.float32
+DISP, WGT, FWD_X, FWD_C, FWD_XC, RET_C, RET_X, RET_EP, RET_G, SHARE, GSUM = range(11)
+
+
+def dot_f32(a, b, dims):
+    return lax.dot_general(a, b, (dims, ((), ())), preferred_element_type=F32)
+
+
+def kernel(
+    n,
+    cap,
+    tok_ref,
+    cot_ref,
+    rw_ref,
+    rt_ref,
+    wg_ref,
+    wu_ref,
+    wd_ref,
+    sd_ref,
+    sh_ref,
+    otok_ref,
+    ow_ref,
+    og_ref,
+    ou_ref,
+    od_ref,
+    ohid_ref,
+    osh_ref,
+    perm,
+    sbuf,
+    abuf,
+    wsend,
+    wrecv,
+    wgu,
+    hw,
+    dgu,
+    part,
+    crecv,
+    keep,
+    xsend,
+    xrecv,
+    rsend,
+    ret,
+    gpart,
+    gcore,
+    gtwo,
+    gx,
+    gsend,
+    gret,
+    ssend,
+    srecv,
+    send_sem,
+    recv_sem,
+):
+    me = lax.axis_index("ep")
+    tp = lax.axis_index("tp")
+    tok_rows, feat = tok_ref.shape
+    top = rt_ref.shape[1]
+    quarter = feat // 4
+    units = wg_ref.shape[1]
+    core_of = lax.rem(tp, 2)
+    half_of = tp // 2
+    tp_c = half_of * 2 + (1 - core_of)
+    tp_x = (1 - half_of) * 2 + core_of
+    tp_xc = (1 - half_of) * 2 + (1 - core_of)
+
+    def copy(kind, at, src_ref, dst_ref, ep_to, tp_to):
+        return pltpu.make_async_remote_copy(
+            src_ref=src_ref,
+            dst_ref=dst_ref,
+            send_sem=send_sem.at[kind, at],
+            recv_sem=recv_sem.at[kind, at],
+            device_id=(ep_to, tp_to),
+            device_id_type=MESH,
+        )
+
+    barrier = pltpu.get_barrier_semaphore()
+    for d in range(1, n):
+        pl.semaphore_signal(
+            barrier, inc=1, device_id=(lax.rem(me + d, n), tp), device_id_type=MESH
+        )
+    for other in (tp_c, tp_x):
+        pl.semaphore_signal(barrier, inc=1, device_id=(me, other), device_id_type=MESH)
+
+    lane = lax.broadcasted_iota(jnp.int32, (tok_rows, 128), 1)
+    named = jnp.zeros((tok_rows, 128), F32)
+    weight_of = jnp.zeros((tok_rows, 128), F32)
+    for k in range(top):
+        hit = rt_ref[:, k : k + 1] == lane
+        named = named + jnp.where(hit, 1.0, 0.0)
+        weight_of = weight_of + jnp.where(hit, rw_ref[:, k : k + 1].astype(BF).astype(F32), 0.0)
+    named_t = named.T
+    weight_t = weight_of.T
+    before = lax.broadcasted_iota(jnp.int32, (tok_rows, tok_rows), 0) < lax.broadcasted_iota(
+        jnp.int32, (tok_rows, tok_rows), 1
+    )
+    rank_t = dot_f32(named_t.astype(BF), jnp.where(before, 1.0, 0.0).astype(BF), ((1,), (0,)))
+    slot = lax.broadcasted_iota(jnp.int32, (cap, tok_rows), 0).astype(F32)
+    wsend[...] = jnp.zeros_like(wsend)
+    gpart[...] = jnp.zeros_like(gpart)
+    for e in range(n):
+        pick = jnp.where(slot == rank_t[e : e + 1, :], named_t[e : e + 1, :], 0.0).astype(BF)
+        perm[e] = pick
+        wrow = jnp.broadcast_to(weight_t[e : e + 1, :], (8, tok_rows)).astype(BF)
+        wsend[e, :, 0:cap] = dot_f32(wrow, pick, ((1,), (1,)))
+    every = perm[...].reshape(n * cap, tok_rows)
+    cols = pl.ds(pl.multiple_of(tp * quarter, quarter), quarter)
+    sbuf[:, 0] = dot_f32(every, tok_ref[:, cols], ((1,), (0,))).astype(BF).reshape(n, cap, quarter)
+    sbuf[:, 1] = dot_f32(every, cot_ref[:, cols], ((1,), (0,))).astype(BF).reshape(n, cap, quarter)
+
+    pl.semaphore_wait(barrier, n + 1)
+
+    def disp(d):
+        to = lax.rem(me + d, n)
+        return copy(DISP, d, sbuf.at[to], abuf.at[me, tp], to, tp)
+
+    def disp_w(d):
+        to = lax.rem(me + d, n)
+        return copy(WGT, d, wsend.at[to], wrecv.at[me], to, tp)
+
+    def disp_in(d):
+        of = lax.rem(me + n - d, n)
+        return copy(DISP, d, abuf.at[of, tp], abuf.at[of, tp], of, tp)
+
+    def disp_w_in(d):
+        of = lax.rem(me + n - d, n)
+        return copy(WGT, d, wrecv.at[of], wrecv.at[of], of, tp)
+
+    def fwd(kind, d, block, to):
+        of = lax.rem(me + n - d, n)
+        return copy(kind, d, abuf.at[of, block], abuf.at[of, block], me, to)
+
+    abuf[me, tp] = sbuf[me]
+    wrecv[me] = wsend[me]
+
+    @pl.loop(1, n)
+    def _(d):
+        disp(d).start()
+        disp_w(d).start()
+
+    fwd(FWD_X, 0, tp, tp_x).start()
+    fwd(FWD_C, 0, tp, tp_c).start()
+
+    wgu[:, 0:units] = wg_ref[...]
+    wgu[:, units : 2 * units] = wu_ref[...]
+    ohid_ref[...] = dot_f32(cot_ref[...], sd_ref[...], ((1,), (0,))).astype(BF)
+    rows_each = feat // n
+    for j in range(n):
+        ssend[j] = dot_f32(
+            cot_ref[:, j * rows_each : (j + 1) * rows_each], sh_ref[...], ((0,), (0,))
+        ).astype(BF)
+
+    @pl.loop(1, n)
+    def _(d):
+        disp_in(d).wait_recv()
+        fwd(FWD_X, d, tp, tp_x).start()
+        fwd(FWD_C, d, tp, tp_c).start()
+
+        @pl.when(d >= 2)
+        def _():
+            fwd(FWD_X, d - 2, tp_x, tp_x).wait_recv()
+            fwd(FWD_XC, d - 2, tp_x, tp_c).start()
+
+    @pl.loop(1, n)
+    def _(d):
+        disp_w_in(d).wait_recv()
+        disp(d).wait_send()
+        disp_w(d).wait_send()
+
+    def share(d):
+        to = lax.rem(me + d, n)
+        return copy(SHARE, d, ssend.at[to], srecv.at[me], to, tp)
+
+    def share_in(d):
+        of = lax.rem(me + n - d, n)
+        return copy(SHARE, d, srecv.at[of], srecv.at[of], of, tp)
+
+    srecv[me] = ssend[me]
+
+    @pl.loop(1, n)
+    def _(d):
+        share(d).start()
+
+    eye = lax.broadcasted_iota(jnp.int32, (cap, cap), 0) == lax.broadcasted_iota(
+        jnp.int32, (cap, cap), 1
+    )
+
+    def to_core(d):
+        of = lax.rem(me + n - d, n)
+        return copy(RET_C, d, part.at[of, 1 - core_of], crecv.at[of], me, tp_c)
+
+    @pl.loop(0, n)
+    def _(d):
+        of = lax.rem(me + n - d, n)
+
+        @pl.when(d >= n - 2)
+        def _():
+            fwd(FWD_X, d, tp_x, tp_x).wait_recv()
+            fwd(FWD_XC, d, tp_x, tp_c).start()
+
+        fwd(FWD_C, d, tp_c, tp_c).wait_recv()
+        fwd(FWD_XC, d, tp_xc, tp_c).wait_recv()
+        both = jnp.zeros((cap, 2 * units), F32)
+        backed = jnp.zeros((cap, units), F32)
+        for b in range(4):
+            at = slice(b * quarter, (b + 1) * quarter)
+            both = both + dot_f32(abuf[of, b, 0], wgu[at, :], ((1,), (0,)))
+            backed = backed + dot_f32(abuf[of, b, 1], wd_ref[:, at], ((1,), (1,)))
+        gate = both[:, 0:units]
+        upper = both[:, units : 2 * units]
+        sigma = jax.nn.sigmoid(gate)
+        active = gate * sigma
+        hidden = (active * upper).astype(BF).astype(F32)
+        wcol = jnp.sum(jnp.where(eye, wrecv[of, 0:1, 0:cap], 0.0), axis=1, keepdims=True)
+        d_hidden = wcol * backed
+        hw[of] = (wcol * hidden).astype(BF)
+        d_both = jnp.concatenate(
+            [
+                (d_hidden * upper * sigma * (1.0 + gate * (1.0 - sigma))).astype(BF),
+                (d_hidden * active).astype(BF),
+            ],
+            axis=1,
+        )
+        dgu[of] = d_both
+        gpart[of, :, 0:cap] = lax.dot_general(
+            jnp.ones((8, units), F32),
+            hidden * backed,
+            (((1,), (1,)), ((), ())),
+            precision=lax.Precision.HIGHEST,
+            preferred_element_type=F32,
+        )
+        for b in range(4):
+            at = slice(b * quarter, (b + 1) * quarter)
+            part[of, b % 2, b // 2] = dot_f32(d_both, wgu[at, :], ((1,), (1,))).astype(BF)
+        to_core(d).start()
+
+    def gate_copy(at, src_ref, dst_ref, to):
+        return copy(GSUM, at, src_ref, dst_ref, me, to)
+
+    gate_copy(0, gpart, gcore, tp_c).start()
+
+    def to_x(d):
+        of = lax.rem(me + n - d, n)
+        return copy(RET_X, d, xsend.at[of], xrecv.at[of], me, tp_x)
+
+    @pl.loop(0, n)
+    def _(d):
+        of = lax.rem(me + n - d, n)
+        to_core(d).wait_recv()
+        xsend[of] = (
+            part[of, core_of, 1 - half_of].astype(F32) + crecv[of, 1 - half_of].astype(F32)
+        ).astype(BF)
+        to_x(d).start()
+        keep[of] = part[of, core_of, half_of].astype(F32) + crecv[of, half_of].astype(F32)
+
+    gate_copy(0, gpart, gcore, tp_c).wait()
+    gtwo[...] = gpart[...] + gcore[...]
+    gate_copy(1, gtwo, gx, tp_x).start()
+
+    d_all = dgu[...].reshape(n * cap, 2 * units)
+    h_all = hw[...].reshape(n * cap, units)
+    for b in range(4):
+        at = slice(b * quarter, (b + 1) * quarter)
+        grad = dot_f32(abuf[:, b, 0].reshape(n * cap, quarter), d_all, ((0,), (0,))).astype(BF)
+        og_ref[at, :] = grad[:, 0:units]
+        ou_ref[at, :] = grad[:, units : 2 * units]
+        od_ref[:, at] = dot_f32(
+            h_all, abuf[:, b, 1].reshape(n * cap, quarter), ((0,), (0,))
+        ).astype(BF)
+
+    gate_copy(1, gtwo, gx, tp_x).wait()
+    gsend[...] = gtwo[...] + gx[...]
+    gret[me] = gsend[me]
+
+    def back(d):
+        to = lax.rem(me + d, n)
+        return copy(RET_EP, d, rsend.at[to], ret.at[me], to, tp)
+
+    def back_g(d):
+        to = lax.rem(me + d, n)
+        return copy(RET_G, d, gsend.at[to], gret.at[me], to, tp)
+
+    def back_in(d):
+        of = lax.rem(me + n - d, n)
+        return copy(RET_EP, d, ret.at[of], ret.at[of], of, tp)
+
+    def back_g_in(d):
+        of = lax.rem(me + n - d, n)
+        return copy(RET_G, d, gret.at[of], gret.at[of], of, tp)
+
+    @pl.loop(1, n)
+    def _(d):
+        back_g(d).start()
+
+    @pl.loop(0, n)
+    def _(d):
+        of = lax.rem(me + n - d, n)
+        to_x(d).wait_recv()
+        total = (keep[of] + xrecv[of].astype(F32)).astype(BF)
+
+        @pl.when(d == 0)
+        def _():
+            ret[me] = total
+
+        @pl.when(d > 0)
+        def _():
+            rsend[of] = total
+            back(lax.rem(n - d, n)).start()
+
+    @pl.loop(1, n)
+    def _(d):
+        share_in(d).wait_recv()
+        back_g_in(d).wait_recv()
+
+    sums = srecv[0].astype(F32)
+    for j in range(1, n):
+        sums = sums + srecv[j].astype(F32)
+    osh_ref[...] = sums
+
+    pieces = []
+    for e in range(n):
+        row = gret[e, :, 0:cap].astype(BF)
+        pieces.append(dot_f32(row, perm[e], ((1,), (0,)))[0:1, :])
+    pieces.append(jnp.zeros((128 - n, tok_rows), F32))
+    values = jnp.concatenate(pieces, axis=0).T
+    for k in range(top):
+        hit = rt_ref[:, k : k + 1] == lane
+        ow_ref[:, k : k + 1] = jnp.sum(jnp.where(hit, values, 0.0), axis=1, keepdims=True)
+
+    @pl.loop(1, n)
+    def _(d):
+        back_in(d).wait_recv()
+
+    otok_ref[...] = dot_f32(
+        perm[...].reshape(n * cap, tok_rows), ret[...].reshape(n * cap, quarter), ((0,), (0,))
+    ).astype(BF)
+
+    @pl.loop(0, n)
+    def _(d):
+        fwd(FWD_X, d, tp, tp_x).wait_send()
+        fwd(FWD_C, d, tp, tp_c).wait_send()
+        fwd(FWD_XC, d, tp_x, tp_c).wait_send()
+        to_core(d).wait_send()
+        to_x(d).wait_send()
+
+    @pl.loop(1, n)
+    def _(d):
+        share(d).wait_send()
+        back(d).wait_send()
+        back_g(d).wait_send()
+
+
+def fused_shards(
+    tokens,
+    cotangent,
+    route_weights,
+    routes,
+    gate_proj,
+    up_proj,
+    down_proj,
+    shared_down,
+    shared_hidden,
+):
+    n = lax.axis_size("ep")
+    tok_rows, feat = tokens.shape
+    units = gate_proj.shape[2]
+    hid = shared_hidden.shape[1]
+    cap = 2 * tok_rows * routes.shape[1] // n
+    quarter = feat // 4
+    out_shape = (
+        jax.ShapeDtypeStruct((tok_rows, quarter), BF),
+        jax.ShapeDtypeStruct(routes.shape, F32),
+        jax.ShapeDtypeStruct((feat, units), BF),
+        jax.ShapeDtypeStruct((feat, units), BF),
+        jax.ShapeDtypeStruct((units, feat), BF),
+        jax.ShapeDtypeStruct((tok_rows, hid), BF),
+        jax.ShapeDtypeStruct((feat // n, hid), F32),
+    )
+    tiles = pltpu.VMEM((n, 8, 128), F32)
+    outs = pl.pallas_call(
+        functools.partial(kernel, n, cap),
+        out_shape=out_shape,
+        in_specs=[pl.BlockSpec(memory_space=pltpu.VMEM)] * 9,
+        out_specs=tuple([pl.BlockSpec(memory_space=pltpu.VMEM)] * 7),
+        scratch_shapes=[
+            pltpu.VMEM((n, cap, tok_rows), BF),
+            pltpu.VMEM((n, 2, cap, quarter), BF),
+            pltpu.VMEM((n, 4, 2, cap, quarter), BF),
+            tiles,
+            tiles,
+            pltpu.VMEM((feat, 2 * units), BF),
+            pltpu.VMEM((n, cap, units), BF),
+            pltpu.VMEM((n, cap, 2 * units), BF),
+            pltpu.VMEM((n, 2, 2, cap, quarter), BF),
+            pltpu.VMEM((n, 2, cap, quarter), BF),
+            pltpu.VMEM((n, cap, quarter), F32),
+            pltpu.VMEM((n, cap, quarter), BF),
+            pltpu.VMEM((n, cap, quarter), BF),
+            pltpu.VMEM((n, cap, quarter), BF),
+            pltpu.VMEM((n, cap, quarter), BF),
+            tiles,
+            tiles,
+            tiles,
+            tiles,
+            tiles,
+            tiles,
+            pltpu.VMEM((n, feat // n, hid), BF),
+            pltpu.VMEM((n, feat // n, hid), BF),
+            pltpu.SemaphoreType.DMA((11, n)),
+            pltpu.SemaphoreType.DMA((11, n)),
+        ],
+        compiler_params=pltpu.CompilerParams(
+            collective_id=0, has_side_effects=True, vmem_limit_bytes=60 * 1024 * 1024
+        ),
+    )(
+        tokens,
+        cotangent,
+        route_weights,
+        routes,
+        gate_proj[0],
+        up_proj[0],
+        down_proj[0],
+        shared_down,
+        shared_hidden,
+    )
+    return outs[0], outs[1], outs[2][None], outs[3][None], outs[4][None], outs[5], outs[6]
+
+
+def shards(*args):
+    tokens, routes, gate_proj = args[0], args[3], args[4]
+    n = lax.axis_size("ep")
+    tok_rows, feat = tokens.shape
+    fits = (
+        gate_proj.shape[0] == 1
+        and lax.axis_size("tp") == 4
+        and tok_rows == 128
+        and n <= 16
+        and (2 * tok_rows * routes.shape[1]) % (16 * n) == 0
+        and 2 * tok_rows * routes.shape[1] // n <= 128
+        and feat % 512 == 0
+        and feat // n % 128 == 0
+    )
+    if fits:
+        return fused_shards(*args)
+    return plain_shards(*args)
+
+
+def plain_shards(
     tokens,
     cotangent,
     route_weights,

time: 199 us -> 89.4 us (0.45)
  Pallas kernels: 0 us -> 78 us
  waiting for transfers between devices: 72.6 us -> 0 us
  blocking collectives: 67.3 us -> 0 us
  matrix products: 19.6 us -> 0 us
  between operations: 14 us -> 0.66 us
  local copies, waits for them, and re-layouts: 16.3 us -> 10.4 us
  starting transfers between devices: 5.68 us -> 0 us
  other arithmetic: 2.98 us -> 0 us
    pallas_call x0 -> x1, Pallas kernels: none -> 78 us  [fused_shards(): pl.pallas_call(functools.partial(kernel, n, cap), out_shape=out_shape, in...]
    all_to_all x4 -> x0, blocking collectives: 61.4 us -> none  [the longest x1 21.7 us: shards(): lax.all_to_all(sent_rows, 'ep', split_axis=0, concat_axis=0, tiled=True)]
    reduce_scatter x2 -> x0, waiting for transfers between devices: 54.1 us -> none  [the longest x1 43 us: shards(): lax.psum_scatter(jnp.einsum('td,th->dh', cotangent, shared_hidden, prefer...]
    dot_general x10 -> x0, matrix products: 19.6 us -> none  [the longest x1 3.13 us: shards(): jnp.einsum('secd,efd->secf', slot_grads, down_proj, preferred_element_typ...]
    all_gather x2 -> x0, waiting for transfers between devices: 11.3 us -> none  [the longest x1 11.3 us: shards(): lax.all_gather(got_grads, 'tp', axis=1, tiled=True)]
    unnamed x20 -> x21, local copies, waits for them, and re-layouts: 2.42 us -> 10.4 us
    all_to_all x1 -> x0, waiting for transfers between devices: 7.17 us -> none  [shards(): lax.all_to_all(input_cols.reshape(filled, quarter), 'ep', split_axis=0, c...]
    gather x4 -> x0, local copies, waits for them, and re-layouts: 7.03 us -> none  [the longest x1 1.97 us: shards(): jnp.take(own_grads, owner_ids, axis=0, mode='fill', fill_value=0)]
  transfers between devices with their start and end apart: 5 -> 0, of which waited for: 4 -> 0; matrix products, arithmetic and copies ran while one was open for 11% -> 0% of each run, Pallas kernels for 0% -> 0%
where the time goes in v1:
time: 89.4 us; the launch traced here: 89.1 us
  Pallas kernels  78 us (87%)
  local copies, waits for them, and re-layouts  10.4 us (12%)
    pallas_call x1, Pallas kernels, fused_shards(): pl.pallas_call(functools.partial(kernel, n, cap), out_shape=out_shape, in...  78 us
    unnamed x21, local copies, waits for them, and re-layouts  10.4 us

profile of v1, /device:TPU:0, one launch (start us, length us, event | category | flops | bytes accessed | tf_op | source)
XLA Modules:
  0.0 89.1 jit_solution(3038324974194814953)
XLA Ops:
  0.6 0.0 copy-start.4
  0.6 0.7 copy-done.4
  1.3 0.0 copy-start.5
  1.3 0.7 copy.16.rw_ref
  2.1 0.0 copy-done.5
  2.1 0.7 copy.17.rt_ref
  2.8 78.0 %shard_map.144 = (bf16[128,512]{1,0:T(8,128)(2,1)}, f32[128,2]{1,0:T(8,128)}, bf16[2048,128]{1,0:T(8,128)(2,1)}, bf16[2048,128]{1,0:T(8,128)(2,1)}, bf16[128,204...) custom-call(bf16[128,2048]{1,0:T(8,128)(2,1)} %tok_ref.1, bf16[128,2048]{1,0:T(8,128)(2,1)} %cot_ref.1, ...), custom_call_target="tpu_custom_call" | custom-call | tf_op jit(solution)/shard_map/pallas_call | solution.py:390
  80.8 1.5 %copy.18 = f32[128,2]{0,1:T(2,128)} copy(f32[128,2]{1,0:T(8,128)} %get-tuple-element.22) | data formatting | bytes 2048
  82.3 1.6 %copy.25 = bf16[128,512]{1,0:T(8,128)(2,1)} copy(bf16[128,512]{1,0:T(8,128)(2,1)} %get-tuple-element.35) | data formatting | bytes 262144
  83.8 0.0 copy-start.1
  83.8 1.9 %copy.26 = bf16[1,2048,128]{2,1,0:T(8,128)(2,1)} copy(bf16[1,2048,128]{2,1,0:T(8,128)(2,1)} %bitcast.11) | data formatting | bytes 1048576
  85.8 0.0 copy-done.1
  85.8 0.0 copy-start
  85.8 0.8 copy.27
  86.6 0.4 copy-done
  87.0 0.0 copy-start.3
  87.0 0.0 copy-start.2
  87.0 0.8 copy.28
  87.8 0.0 copy-done.3
  87.8 0.6 copy.29
  88.4 0.0 copy-done.2
  88.4 0.7 copy.30
Async XLA Ops:
  0.6 0.7 copy-start.4
  1.3 0.7 copy-start.5
  83.8 1.9 %copy-start.1 = (bf16[2048,128]{1,0:T(8,128)(2,1)S(1)}, bf16[2048,128]{1,0:T(8,128)(2,1)}, u32[]{:S(2)}) copy-start(bf16[2048,128]{1,0:T(8,128)(2,1)} %get-tuple-element.17) | copy-start | bytes 1572868
  85.8 1.2 %copy-start = (bf16[128,2048]{1,0:T(8,128)(2,1)S(1)}, bf16[128,2048]{1,0:T(8,128)(2,1)}, u32[]{:S(2)}) copy-start(bf16[128,2048]{1,0:T(8,128)(2,1)} %get-tuple-element.18) | copy-start | bytes 1572868
  87.0 0.8 copy-start.3
  87.0 1.4 %copy-start.2 = (f32[256,128]{1,0:T(8,128)S(1)}, f32[256,128]{1,0:T(8,128)}, u32[]{:S(2)}) copy-start(f32[256,128]{1,0:T(8,128)} %get-tuple-element.41) | copy-start | bytes 393220

commit v2 on v1

--- a/solution.py
+++ b/solution.py
@@ -10,7 +10,7 @@
 MESH = pl.DeviceIdType.MESH
 BF = jnp.bfloat16
 F32 = jnp.float32
-DISP, WGT, FWD_X, FWD_C, FWD_XC, RET_C, RET_X, RET_EP, RET_G, SHARE, GSUM = range(11)
+DISP, WGT, FWD_X, FWD_C, FWD_XC, RET_C, RET_X, RET_EP, RET_G, SHARE, GSUM, PAIR = range(12)
 
 
 def dot_f32(a, b, dims):
@@ -42,6 +42,9 @@
     wsend,
     wrecv,
     wgu,
+    wdv,
+    sdv,
+    gradv,
     hw,
     dgu,
     part,
@@ -58,14 +61,18 @@
     gsend,
     gret,
     ssend,
+    spair,
+    ssum,
     srecv,
     send_sem,
     recv_sem,
+    load_sem,
+    store_sem,
 ):
     me = lax.axis_index("ep")
     tp = lax.axis_index("tp")
     tok_rows, feat = tok_ref.shape
-    top = rt_ref.shape[1]
+    top = rt_ref.shape[0]
     quarter = feat // 4
     units = wg_ref.shape[1]
     core_of = lax.rem(tp, 2)
@@ -84,23 +91,30 @@
             device_id_type=MESH,
         )
 
+    loads = [
+        pltpu.make_async_copy(wg_ref, wgu.at[:, pl.ds(0, units)], load_sem.at[0]),
+        pltpu.make_async_copy(wu_ref, wgu.at[:, pl.ds(units, units)], load_sem.at[1]),
+        pltpu.make_async_copy(wd_ref, wdv, load_sem.at[2]),
+        pltpu.make_async_copy(sd_ref, sdv, load_sem.at[3]),
+    ]
     barrier = pltpu.get_barrier_semaphore()
     for d in range(1, n):
         pl.semaphore_signal(
-            barrier, inc=1, device_id=(lax.rem(me + d, n), tp), device_id_type=MESH
+            barrier, inc=1, device_id=(jnp.bitwise_xor(me, d), tp), device_id_type=MESH
         )
     for other in (tp_c, tp_x):
         pl.semaphore_signal(barrier, inc=1, device_id=(me, other), device_id_type=MESH)
 
-    lane = lax.broadcasted_iota(jnp.int32, (tok_rows, 128), 1)
-    named = jnp.zeros((tok_rows, 128), F32)
-    weight_of = jnp.zeros((tok_rows, 128), F32)
+    for load in loads:
+        load.start()
+
+    names = lax.broadcasted_iota(jnp.int32, (128, tok_rows), 0)
+    named_t = jnp.zeros((128, tok_rows), F32)
+    weight_t = jnp.zeros((128, tok_rows), F32)
     for k in range(top):
-        hit = rt_ref[:, k : k + 1] == lane
-        named = named + jnp.where(hit, 1.0, 0.0)
-        weight_of = weight_of + jnp.where(hit, rw_ref[:, k : k + 1].astype(BF).astype(F32), 0.0)
-    named_t = named.T
-    weight_t = weight_of.T
+        hit = rt_ref[k : k + 1, :] == names
+        named_t = named_t + jnp.where(hit, 1.0, 0.0)
+        weight_t = weight_t + jnp.where(hit, rw_ref[k : k + 1, :].astype(BF).astype(F32), 0.0)
     before = lax.broadcasted_iota(jnp.int32, (tok_rows, tok_rows), 0) < lax.broadcasted_iota(
         jnp.int32, (tok_rows, tok_rows), 1
     )
@@ -121,93 +135,82 @@
     pl.semaphore_wait(barrier, n + 1)
 
     def disp(d):
-        to = lax.rem(me + d, n)
+        to = jnp.bitwise_xor(me, d)
         return copy(DISP, d, sbuf.at[to], abuf.at[me, tp], to, tp)
 
     def disp_w(d):
-        to = lax.rem(me + d, n)
+        to = jnp.bitwise_xor(me, d)
         return copy(WGT, d, wsend.at[to], wrecv.at[me], to, tp)
 
     def disp_in(d):
-        of = lax.rem(me + n - d, n)
+        of = jnp.bitwise_xor(me, d)
         return copy(DISP, d, abuf.at[of, tp], abuf.at[of, tp], of, tp)
 
     def disp_w_in(d):
-        of = lax.rem(me + n - d, n)
+        of = jnp.bitwise_xor(me, d)
         return copy(WGT, d, wrecv.at[of], wrecv.at[of], of, tp)
 
     def fwd(kind, d, block, to):
-        of = lax.rem(me + n - d, n)
+        of = jnp.bitwise_xor(me, d)
         return copy(kind, d, abuf.at[of, block], abuf.at[of, block], me, to)
 
     abuf[me, tp] = sbuf[me]
     wrecv[me] = wsend[me]
 
-    @pl.loop(1, n)
-    def _(d):
+    half = n // 2
+    for d in [half, half + 1] + list(range(1, half)):
         disp(d).start()
+    for d in range(1, n):
         disp_w(d).start()
 
-    fwd(FWD_X, 0, tp, tp_x).start()
-    fwd(FWD_C, 0, tp, tp_c).start()
-
-    wgu[:, 0:units] = wg_ref[...]
-    wgu[:, units : 2 * units] = wu_ref[...]
-    ohid_ref[...] = dot_f32(cot_ref[...], sd_ref[...], ((1,), (0,))).astype(BF)
+    for load in loads:
+        load.wait()
+    ohid_ref[...] = dot_f32(cot_ref[...], sdv[...], ((1,), (0,))).astype(BF)
     rows_each = feat // n
     for j in range(n):
-        ssend[j] = dot_f32(
+        ssend[j % 2, j // 2] = dot_f32(
             cot_ref[:, j * rows_each : (j + 1) * rows_each], sh_ref[...], ((0,), (0,))
         ).astype(BF)
-
-    @pl.loop(1, n)
-    def _(d):
-        disp_in(d).wait_recv()
+    odd = lax.rem(me, 2)
+    pair = copy(PAIR, 0, ssend.at[1 - odd], spair, jnp.bitwise_xor(me, 1), tp)
+    pair.start()
+
+    def share(d):
+        to = jnp.bitwise_xor(me, 2 * d)
+        return copy(SHARE, d, ssum.at[to // 2], srecv.at[me // 2], to, tp)
+
+    def share_in(d):
+        of = jnp.bitwise_xor(me, 2 * d)
+        return copy(SHARE, d, srecv.at[of // 2], srecv.at[of // 2], of, tp)
+
+    eye = lax.broadcasted_iota(jnp.int32, (cap, cap), 0) == lax.broadcasted_iota(
+        jnp.int32, (cap, cap), 1
+    )
+
+    def to_core(d):
+        of = jnp.bitwise_xor(me, d)
+        return copy(RET_C, d, part.at[of, 1 - core_of], crecv.at[of], me, tp_c)
+
+    def arrive(d):
+        @pl.when(d > 0)
+        def _():
+            disp_in(d).wait_recv()
+            disp_w_in(d).wait_recv()
+
         fwd(FWD_X, d, tp, tp_x).start()
         fwd(FWD_C, d, tp, tp_c).start()
 
-        @pl.when(d >= 2)
-        def _():
-            fwd(FWD_X, d - 2, tp_x, tp_x).wait_recv()
-            fwd(FWD_XC, d - 2, tp_x, tp_c).start()
-
-    @pl.loop(1, n)
-    def _(d):
-        disp_w_in(d).wait_recv()
-        disp(d).wait_send()
-        disp_w(d).wait_send()
-
-    def share(d):
-        to = lax.rem(me + d, n)
-        return copy(SHARE, d, ssend.at[to], srecv.at[me], to, tp)
-
-    def share_in(d):
-        of = lax.rem(me + n - d, n)
-        return copy(SHARE, d, srecv.at[of], srecv.at[of], of, tp)
-
-    srecv[me] = ssend[me]
-
-    @pl.loop(1, n)
-    def _(d):
-        share(d).start()
-
-    eye = lax.broadcasted_iota(jnp.int32, (cap, cap), 0) == lax.broadcasted_iota(
-        jnp.int32, (cap, cap), 1
-    )
-
-    def to_core(d):
-        of = lax.rem(me + n - d, n)
-        return copy(RET_C, d, part.at[of, 1 - core_of], crecv.at[of], me, tp_c)
-
-    @pl.loop(0, n)
-    def _(d):
-        of = lax.rem(me + n - d, n)
-
-        @pl.when(d >= n - 2)
-        def _():
-            fwd(FWD_X, d, tp_x, tp_x).wait_recv()
-            fwd(FWD_XC, d, tp_x, tp_c).start()
-
+        @pl.when((d >= half) & (d < n - 2))
+        def _():
+            disp(d).wait_send()
+            disp(d + 2).start()
+
+    def pass_core(d):
+        fwd(FWD_X, d, tp_x, tp_x).wait_recv()
+        fwd(FWD_XC, d, tp_x, tp_c).start()
+
+    def compute(d):
+        of = jnp.bitwise_xor(me, d)
         fwd(FWD_C, d, tp_c, tp_c).wait_recv()
         fwd(FWD_XC, d, tp_xc, tp_c).wait_recv()
         both = jnp.zeros((cap, 2 * units), F32)
@@ -215,7 +218,7 @@
         for b in range(4):
             at = slice(b * quarter, (b + 1) * quarter)
             both = both + dot_f32(abuf[of, b, 0], wgu[at, :], ((1,), (0,)))
-            backed = backed + dot_f32(abuf[of, b, 1], wd_ref[:, at], ((1,), (1,)))
+            backed = backed + dot_f32(abuf[of, b, 1], wdv[:, at], ((1,), (1,)))
         gate = both[:, 0:units]
         upper = both[:, units : 2 * units]
         sigma = jax.nn.sigmoid(gate)
@@ -247,15 +250,12 @@
     def gate_copy(at, src_ref, dst_ref, to):
         return copy(GSUM, at, src_ref, dst_ref, me, to)
 
-    gate_copy(0, gpart, gcore, tp_c).start()
-
     def to_x(d):
-        of = lax.rem(me + n - d, n)
+        of = jnp.bitwise_xor(me, d)
         return copy(RET_X, d, xsend.at[of], xrecv.at[of], me, tp_x)
 
-    @pl.loop(0, n)
-    def _(d):
-        of = lax.rem(me + n - d, n)
+    def core_sum(d):
+        of = jnp.bitwise_xor(me, d)
         to_core(d).wait_recv()
         xsend[of] = (
             part[of, core_of, 1 - half_of].astype(F32) + crecv[of, 1 - half_of].astype(F32)
@@ -263,6 +263,73 @@
         to_x(d).start()
         keep[of] = part[of, core_of, half_of].astype(F32) + crecv[of, half_of].astype(F32)
 
+    def back(d):
+        to = jnp.bitwise_xor(me, d)
+        return copy(RET_EP, d, rsend.at[to], ret.at[me], to, tp)
+
+    def back_g(d):
+        to = jnp.bitwise_xor(me, d)
+        return copy(RET_G, d, gsend.at[to], gret.at[me], to, tp)
+
+    def back_in(d):
+        of = jnp.bitwise_xor(me, d)
+        return copy(RET_EP, d, ret.at[of], ret.at[of], of, tp)
+
+    def back_g_in(d):
+        of = jnp.bitwise_xor(me, d)
+        return copy(RET_G, d, gret.at[of], gret.at[of], of, tp)
+
+    def return_block(d):
+        of = jnp.bitwise_xor(me, d)
+        to_x(d).wait_recv()
+        total = (keep[of] + xrecv[of].astype(F32)).astype(BF)
+
+        @pl.when(d == 0)
+        def _():
+            ret[me] = total
+
+        @pl.when(d > 0)
+        def _():
+            rsend[of] = total
+            back(d).start()
+
+    lag = 4
+
+    @pl.loop(0, n + 2)
+    def _(t):
+        @pl.when(t < n)
+        def _():
+            arrive(t)
+
+        @pl.when((t >= 1) & (t <= n))
+        def _():
+            compute(t - 1)
+
+        @pl.when(t >= 2)
+        def _():
+            core_sum(t - 2)
+
+        @pl.when(t >= lag)
+        def _():
+            return_block(t - lag)
+
+        @pl.when(t < n)
+        def _():
+            pass_core(t)
+
+        @pl.when(t == half)
+        def _():
+            pair.wait_recv()
+            for z in range(half):
+                ssum[z] = (ssend[odd, z].astype(F32) + spair[z].astype(F32)).astype(BF)
+            srecv[me // 2] = ssum[me // 2]
+
+        @pl.when(t == n - 1)
+        def _():
+            for other in range(1, half):
+                share(other).start()
+
+    gate_copy(0, gpart, gcore, tp_c).start()
     gate_copy(0, gpart, gcore, tp_c).wait()
     gtwo[...] = gpart[...] + gcore[...]
     gate_copy(1, gtwo, gx, tp_x).start()
@@ -272,58 +339,40 @@
     for b in range(4):
         at = slice(b * quarter, (b + 1) * quarter)
         grad = dot_f32(abuf[:, b, 0].reshape(n * cap, quarter), d_all, ((0,), (0,))).astype(BF)
-        og_ref[at, :] = grad[:, 0:units]
-        ou_ref[at, :] = grad[:, units : 2 * units]
-        od_ref[:, at] = dot_f32(
+        gradv[0, at, :] = grad[:, 0:units]
+        gradv[1, at, :] = grad[:, units : 2 * units]
+        wdv[:, at] = dot_f32(
             h_all, abuf[:, b, 1].reshape(n * cap, quarter), ((0,), (0,))
         ).astype(BF)
+
+    stores = [
+        pltpu.make_async_copy(gradv.at[0], og_ref, store_sem.at[0]),
+        pltpu.make_async_copy(gradv.at[1], ou_ref, store_sem.at[1]),
+        pltpu.make_async_copy(wdv, od_ref, store_sem.at[2]),
+    ]
+    for store in stores:
+        store.start()
 
     gate_copy(1, gtwo, gx, tp_x).wait()
     gsend[...] = gtwo[...] + gx[...]
     gret[me] = gsend[me]
 
-    def back(d):
-        to = lax.rem(me + d, n)
-        return copy(RET_EP, d, rsend.at[to], ret.at[me], to, tp)
-
-    def back_g(d):
-        to = lax.rem(me + d, n)
-        return copy(RET_G, d, gsend.at[to], gret.at[me], to, tp)
-
-    def back_in(d):
-        of = lax.rem(me + n - d, n)
-        return copy(RET_EP, d, ret.at[of], ret.at[of], of, tp)
-
-    def back_g_in(d):
-        of = lax.rem(me + n - d, n)
-        return copy(RET_G, d, gret.at[of], gret.at[of], of, tp)
-
     @pl.loop(1, n)
     def _(d):
         back_g(d).start()
 
-    @pl.loop(0, n)
-    def _(d):
-        of = lax.rem(me + n - d, n)
-        to_x(d).wait_recv()
-        total = (keep[of] + xrecv[of].astype(F32)).astype(BF)
-
-        @pl.when(d == 0)
-        def _():
-            ret[me] = total
-
-        @pl.when(d > 0)
-        def _():
-            rsend[of] = total
-            back(lax.rem(n - d, n)).start()
+    for d in range(n + 2 - lag, n):
+        return_block(jnp.int32(d))
 
     @pl.loop(1, n)
     def _(d):
+        back_g_in(d).wait_recv()
+
+    for d in range(1, half):
         share_in(d).wait_recv()
-        back_g_in(d).wait_recv()
 
     sums = srecv[0].astype(F32)
-    for j in range(1, n):
+    for j in range(1, half):
         sums = sums + srecv[j].astype(F32)
     osh_ref[...] = sums
 
@@ -332,10 +381,10 @@
         row = gret[e, :, 0:cap].astype(BF)
         pieces.append(dot_f32(row, perm[e], ((1,), (0,)))[0:1, :])
     pieces.append(jnp.zeros((128 - n, tok_rows), F32))
-    values = jnp.concatenate(pieces, axis=0).T
+    values = jnp.concatenate(pieces, axis=0)
     for k in range(top):
-        hit = rt_ref[:, k : k + 1] == lane
-        ow_ref[:, k : k + 1] = jnp.sum(jnp.where(hit, values, 0.0), axis=1, keepdims=True)
+        hit = rt_ref[k : k + 1, :] == names
+        ow_ref[k : k + 1, :] = jnp.sum(jnp.where(hit, values, 0.0), axis=0, keepdims=True)
 
     @pl.loop(1, n)
     def _(d):
@@ -344,6 +393,9 @@
     otok_ref[...] = dot_f32(
         perm[...].reshape(n * cap, tok_rows), ret[...].reshape(n * cap, quarter), ((0,), (0,))
     ).astype(BF)
+
+    for store in stores:
+        store.wait()
 
     @pl.loop(0, n)
     def _(d):
@@ -355,9 +407,43 @@
 
     @pl.loop(1, n)
     def _(d):
-        share(d).wait_send()
         back(d).wait_send()
         back_g(d).wait_send()
+        disp_w(d).wait_send()
+
+    for d in list(range(1, half)) + [n - 2, n - 1]:
+        disp(d).wait_send()
+    for d in range(1, half):
+        share(d).wait_send()
+    pair.wait_send()
+
+
+def pass_on(*refs):
+    count = (len(refs) - 2) // 3
+    ins, outs, held = refs[:count], refs[count : 2 * count], refs[2 * count : 3 * count]
+    in_sem, out_sem = refs[-2:]
+    loads = [pltpu.make_async_copy(ins[i], held[i], in_sem.at[i]) for i in range(count)]
+    stores = [pltpu.make_async_copy(held[i], outs[i], out_sem.at[i]) for i in range(count)]
+    for load in loads:
+        load.start()
+    for load, store in zip(loads, stores):
+        load.wait()
+        store.start()
+    for store in stores:
+        store.wait()
+
+
+def hand_over(arrays):
+    count = len(arrays)
+    hbm = pl.BlockSpec(memory_space=pl.ANY)
+    return pl.pallas_call(
+        pass_on,
+        out_shape=tuple(jax.ShapeDtypeStruct(a.shape, a.dtype) for a in arrays),
+        in_specs=[hbm] * count,
+        out_specs=tuple([hbm] * count),
+        scratch_shapes=[pltpu.VMEM(a.shape, a.dtype) for a in arrays]
+        + [pltpu.SemaphoreType.DMA((count,))] * 2,
+    )(*arrays)
 
 
 def fused_shards(
@@ -379,7 +465,7 @@
     quarter = feat // 4
     out_shape = (
         jax.ShapeDtypeStruct((tok_rows, quarter), BF),
-        jax.ShapeDtypeStruct(routes.shape, F32),
+        jax.ShapeDtypeStruct(routes.shape[::-1], F32),
         jax.ShapeDtypeStruct((feat, units), BF),
         jax.ShapeDtypeStruct((feat, units), BF),
         jax.ShapeDtypeStruct((units, feat), BF),
@@ -387,11 +473,13 @@
         jax.ShapeDtypeStruct((feat // n, hid), F32),
     )
     tiles = pltpu.VMEM((n, 8, 128), F32)
+    vmem = pl.BlockSpec(memory_space=pltpu.VMEM)
+    hbm = pl.BlockSpec(memory_space=pl.ANY)
     outs = pl.pallas_call(
         functools.partial(kernel, n, cap),
         out_shape=out_shape,
-        in_specs=[pl.BlockSpec(memory_space=pltpu.VMEM)] * 9,
-        out_specs=tuple([pl.BlockSpec(memory_space=pltpu.VMEM)] * 7),
+        in_specs=[vmem] * 4 + [hbm] * 4 + [vmem],
+        out_specs=(vmem, vmem, hbm, hbm, hbm, vmem, vmem),
         scratch_shapes=[
             pltpu.VMEM((n, cap, tok_rows), BF),
             pltpu.VMEM((n, 2, cap, quarter), BF),
@@ -399,6 +487,9 @@
             tiles,
             tiles,
             pltpu.VMEM((feat, 2 * units), BF),
+            pltpu.VMEM((units, feat), BF),
+            pltpu.VMEM((feat, hid), BF),
+            pltpu.VMEM((2, feat, units), BF),
             pltpu.VMEM((n, cap, units), BF),
             pltpu.VMEM((n, cap, 2 * units), BF),
             pltpu.VMEM((n, 2, 2, cap, quarter), BF),
@@ -414,10 +505,14 @@
             tiles,
             tiles,
             tiles,
-            pltpu.VMEM((n, feat // n, hid), BF),
-            pltpu.VMEM((n, feat // n, hid), BF),
-            pltpu.SemaphoreType.DMA((11, n)),
-            pltpu.SemaphoreType.DMA((11, n)),
+            pltpu.VMEM((2, n // 2, feat // n, hid), BF),
+            pltpu.VMEM((n // 2, feat // n, hid), BF),
+            pltpu.VMEM((n // 2, feat // n, hid), BF),
+            pltpu.VMEM((n // 2, feat // n, hid), BF),
+            pltpu.SemaphoreType.DMA((12, n)),
+            pltpu.SemaphoreType.DMA((12, n)),
+            pltpu.SemaphoreType.DMA((4,)),
+            pltpu.SemaphoreType.DMA((3,)),
         ],
         compiler_params=pltpu.CompilerParams(
             collective_id=0, has_side_effects=True, vmem_limit_bytes=60 * 1024 * 1024
@@ -425,15 +520,16 @@
     )(
         tokens,
         cotangent,
-        route_weights,
-        routes,
+        route_weights.T,
+        routes.T,
         gate_proj[0],
         up_proj[0],
         down_proj[0],
         shared_down,
         shared_hidden,
     )
-    return outs[0], outs[1], outs[2][None], outs[3][None], outs[4][None], outs[5], outs[6]
+    outs = hand_over(outs)
+    return outs[0], outs[1].T, outs[2][None], outs[3][None], outs[4][None], outs[5], outs[6]
 
 
 def shards(*args):
@@ -444,7 +540,7 @@
         gate_proj.shape[0] == 1
         and lax.axis_size("tp") == 4
         and tok_rows == 128
-        and n <= 16
+        and n in (8, 16)
         and (2 * tok_rows * routes.shape[1]) % (16 * n) == 0
         and 2 * tok_rows * routes.shape[1] // n <= 128
         and feat % 512 == 0

time: 89.4 us -> 68.8 us (0.77)
  local copies, waits for them, and re-layouts: 10.4 us -> 0 us
  Pallas kernels: 78 us -> 67.8 us
    pallas_call x1, Pallas kernels: 78 us -> 65.4 us  [fused_shards(): pl.pallas_call(functools.partial(kernel, n, cap), out_shape=out_shape, in...]
    unnamed x21 -> x0, local copies, waits for them, and re-layouts: 10.4 us -> none
    pallas_call x0 -> x1, Pallas kernels: none -> 2.43 us  [hand_over(): pl.pallas_call(pass_on, out_shape=tuple((jax.ShapeDtypeStruct(a.shape, a....]
where the time goes in v2:
time: 68.8 us; the launch traced here: 68.4 us
  Pallas kernels  67.8 us (99%)
    pallas_call x1, Pallas kernels, fused_shards(): pl.pallas_call(functools.partial(kernel, n, cap), out_shape=out_shape, in...  65.4 us
    pallas_call x1, Pallas kernels, hand_over(): pl.pallas_call(pass_on, out_shape=tuple((jax.ShapeDtypeStruct(a.shape, a....  2.43 us

profile of v2, /device:TPU:0, one launch (start us, length us, event | category | flops | bytes accessed | tf_op | source)
XLA Modules:
  0.0 68.4 jit_solution(9844307127971570798)
XLA Ops:
  0.6 65.4 %shard_map.144 = (bf16[128,512]{1,0:T(8,128)(2,1)}, f32[2,128]{1,0:T(2,128)}, bf16[2048,128]{1,0:T(8,128)(2,1)}, bf16[2048,128]{1,0:T(8,128)(2,1)}, bf16[128,204...) custom-call(bf16[128,2048]{1,0:T(8,128)(2,1)} %tok_ref.1, bf16[128,2048]{1,0:T(8,128)(2,1)} %cot_ref.1, ...), custom_call_target="tpu_custom_call" | custom-call | tf_op jit(solution)/shard_map/pallas_call | solution.py:478
  66.0 2.4 %shard_map.145 = (bf16[128,512]{1,0:T(8,128)(2,1)}, f32[2,128]{1,0:T(2,128)}, bf16[2048,128]{1,0:T(8,128)(2,1)}, bf16[2048,128]{1,0:T(8,128)(2,1)}, bf16[128,204...) custom-call(bf16[128,512]{1,0:T(8,128)(2,1)} %get-tuple-element.21.refs_0_, ...), custom_call_target="tpu_custom_call" | custom-call | tf_op jit(solution)/shard_map/pallas_call | solution.py:439
